TPU v7x, 32 devices: a whole 2x2x4 slice. The times are simulated.
32 devices in a mesh: ep: 8 (over z, core), tp: 4 (over y, x).
Axes of the slice: x: 2, y: 2, z: 4, core: 2. Of those that a mesh axis runs over, the one named last changes fastest.
Arguments:
- resid: bfloat16 [64, 2048], P('ep', 'tp'), may hold values from -6 to 6
- attn_gain: float32 [2048], replicated, may hold values from 0.1 to 1.9
- w_query: bfloat16 [2048, 1024], P(None, 'tp'), may hold values from -0.125 to 0.125
- w_key: bfloat16 [2048, 1024], P(None, 'tp'), may hold values from -0.125 to 0.125
- w_value: bfloat16 [2048, 1024], P(None, 'tp'), may hold values from -0.125 to 0.125
- key_cache: bfloat16 [64, 16, 64, 1024], P('ep', 'tp'), may hold values from -6 to 6
- value_cache: bfloat16 [64, 16, 64, 1024], P('ep', 'tp'), may hold values from -19 to 19
- key_bias: float32 [64, 16, 1024], P('ep', 'tp'), may hold values from -10.2 to 0
- lengths: int32 [64], P('ep'), may hold values from 1 to 1024
- mix_gain: float32 [1024], P('tp'), may hold values from 0.1 to 1.9
- w_out: bfloat16 [1024, 2048], P('tp'), may hold values from -0.1875 to 0.1875
- ffn_gain: float32 [2048], replicated, may hold values from 0.1 to 1.9
- route_experts: int32 [64, 4], P('ep'), may hold values from 0 to 7, all different within a row; in each aligned block of 8 rows (0 to 7, 8 to 15, ...) at most 8 rows name the same one
- route_weights: float32 [64, 4], P('ep'), may hold values from 0.05 to 1
- w_gate: bfloat16 [8, 2048, 2048], P('ep', None, 'tp'), may hold values from -0.3125 to 0.3125
- w_up: bfloat16 [8, 2048, 2048], P('ep', None, 'tp'), may hold values from -0.3125 to 0.3125
- w_down: bfloat16 [8, 2048, 2048], P('ep', 'tp'), may hold values from -0.0546875 to 0.0546875
Outputs:
- mixed: bfloat16 [64, 2048], P('ep', 'tp')
- new_keys: bfloat16 [64, 1024], P('ep', 'tp')
- new_values: bfloat16 [64, 1024], P('ep', 'tp')
Inputs may be any that keep to these rules, and one draw needn't show every extreme that they name: `route_experts`: each row names 4 different experts. Within the rows of one device (aligned blocks of 8 rows) no expert is named more than 8 times, a bound that some block reaches.
All inputs are finite; a program needn't handle non-finite values.
Results may differ from a plain program's by a relative error of at most 0.018.
Values may be sent and summed in bfloat16 or wider, within the bound.
A program may use at most 64 MiB of HBM per device.

v0:
```python
import functools

import jax
import jax.numpy as jnp
from jax import lax
from jax.experimental import pallas as pl
from jax.experimental.pallas import tpu as pltpu
from jax.sharding import PartitionSpec as P

eps = 1e-06
limit = 7.0
alpha = 1.702
MESH = pl.DeviceIdType.MESH
F32 = jnp.float32
BF16 = jnp.bfloat16


def mm(a, b):
    return jnp.dot(a, b, preferred_element_type=F32)


def mm_nt(a, b):
    return lax.dot_general(a, b, (((1,), (1,)), ((), ())), preferred_element_type=F32)


def layer(
    tp, ep, heads, width,
    h_resid, h_attn_gain, h_lengths, h_mix_gain, h_ffn_gain, h_experts, h_weights,
    h_wq, h_key, h_bias, h_value, h_wo, h_gate, h_up, h_wk, h_wv, h_down,
    mixed, new_keys, new_values,
    resid, attn_gain, lengths, mix_gain, ffn_gain, route_experts, route_weights,
    wq, key, bias, value, wo, gate_w, up_w, wk, wv, down_w,
    gathered, bias_rows, branch, squares, mid, tokens, pieces, arrived, outs, back,
    load_sem, res_send, res_recv, br_send, br_recv, sq_send, sq_recv,
    tok_send, tok_recv, fwd_send, fwd_recv, down_send, down_recv, ret_send, ret_recv,
):
    t = lax.axis_index("tp")
    e = lax.axis_index("ep")
    chips = ep // 2
    z, core = e // 2, lax.rem(e, 2)
    seqs, shard = resid.shape
    model = tp * shard
    span = heads * width
    rows = seqs * heads
    cache = key.shape[1]

    def tp_peer(d):
        return {"tp": lax.rem(t + d, tp)}

    def ep_peer(d):
        return {"ep": lax.rem(e + d, ep)}

    def remote(src, dst, send, recv, device):
        return pltpu.make_async_remote_copy(
            src_ref=src, dst_ref=dst, send_sem=send, recv_sem=recv, device_id=device, device_id_type=MESH
        )

    barrier = pltpu.get_barrier_semaphore()
    for d in range(1, tp):
        pl.semaphore_signal(barrier, inc=1, device_id=tp_peer(d), device_id_type=MESH)
    for d in range(1, ep):
        pl.semaphore_signal(barrier, inc=1, device_id=ep_peer(d), device_id_type=MESH)
    loads = []
    for i, (src, dst) in enumerate((
        (h_resid, resid), (h_attn_gain, attn_gain), (h_wq, wq), (h_lengths, lengths), (h_key, key), (h_bias, bias), (h_value, value),
        (h_mix_gain, mix_gain), (h_wo, wo), (h_ffn_gain, ffn_gain), (h_experts, route_experts), (h_weights, route_weights),
        (h_gate.at[0], gate_w), (h_up.at[0], up_w), (h_wk, wk), (h_wv, wv), (h_down.at[0], down_w),
    )):
        copy = pltpu.make_async_copy(src, dst, load_sem.at[i])
        copy.start()
        loads.append(copy)
    (
        l_resid, l_attn, l_wq, l_length, l_key, l_bias, l_value, l_mix, l_wo, l_ffn, l_experts, l_weights,
        l_gate, l_up, l_wk, l_wv, l_down,
    ) = loads

    l_resid.wait()
    pl.semaphore_wait(barrier, tp + ep - 2)

    sent = []
    res = []
    for d in range(1, tp):
        copy = remote(resid, gathered.at[t], res_send.at[d], res_recv.at[d], tp_peer(d))
        copy.start()
        res.append(copy)
    sent += res
    gathered[t] = resid[...]

    l_bias.wait()
    l_length.wait()
    for n in range(seqs):
        bias_rows[pl.ds(n * heads, heads), :] = bias[n]
    row = lax.broadcasted_iota(jnp.int32, (rows, 1), 0)
    length = jnp.zeros((rows, 1), jnp.int32)
    for n in range(seqs):
        length = jnp.where(row // heads == n, lengths[n], length)
    live = lax.broadcasted_iota(jnp.int32, (rows, cache), 1) < length
    own_row = lax.broadcasted_iota(jnp.int32, (rows, span), 0)
    own_head = lax.broadcasted_iota(jnp.int32, (rows, span), 1) // width
    repeat = (
        lax.broadcasted_iota(jnp.int32, (rows, seqs), 0) // heads
        == lax.broadcasted_iota(jnp.int32, (rows, seqs), 1)
    ).astype(F32).astype(BF16)
    block = min(256, cache)
    blocks = cache // block
    lower = (
        lax.broadcasted_iota(jnp.int32, (block, block), 0)
        >= lax.broadcasted_iota(jnp.int32, (block, block), 1)
    ).astype(F32).astype(BF16)

    l_attn.wait()
    l_wq.wait()
    l_key.wait()
    for copy in res:
        copy.wait_recv()
    whole = jnp.concatenate([gathered[j].astype(F32) for j in range(tp)], axis=1)
    normed_in = (
        whole * lax.rsqrt(jnp.mean(whole * whole, axis=1, keepdims=True) + eps) * attn_gain[...]
    ).astype(BF16)
    query = mm(normed_in, wq[...]).astype(BF16)

    spread = mm(repeat, query)
    scores = bias_rows[...]
    total = jnp.zeros((rows, cache), F32)
    for n in range(seqs):
        masked = jnp.where(own_row == n * heads + own_head, spread, 0.0).astype(BF16)
        total = total + mm(masked, key[pl.ds(n * span, span), :])
    scores = total * width ** (-0.5) + scores
    soft = jnp.maximum(scores, 0.0) + jnp.log1p(jnp.exp(-jnp.abs(scores)))
    soft = jnp.where(live, soft, 0.0)
    stacked = jnp.concatenate([soft[:, b * block:(b + 1) * block] for b in range(blocks)], axis=0)
    high = stacked.astype(BF16)
    rest = stacked - high.astype(F32)
    middle_part = rest.astype(BF16)
    low = (rest - middle_part.astype(F32)).astype(BF16)
    within = mm(high, lower) + mm(middle_part, lower) + mm(low, lower)
    later = jnp.zeros((rows, 1), F32)
    suffix = [None] * blocks
    for b in reversed(range(blocks)):
        part = within[b * rows:(b + 1) * rows]
        suffix[b] = part + later
        later = later + part[:, 0:1]
    suffix = jnp.concatenate(suffix, axis=1)
    stick = jnp.where(live, jnp.exp(scores - suffix), 0.0).astype(BF16)

    l_value.wait()
    seq_row = lax.broadcasted_iota(jnp.int32, (seqs, span), 0)
    attended = jnp.zeros((seqs, span), F32)
    for n in range(seqs):
        product = mm_nt(stick, value[pl.ds(n * span, span), :])
        product = jnp.where(own_row == n * heads + own_head, product, 0.0)
        attended = jnp.where(seq_row == n, jnp.sum(product, axis=0, keepdims=True), attended)

    squares[t] = jnp.broadcast_to(jnp.sum(attended * attended, axis=1, keepdims=True), (seqs, 128))
    exchange = []
    for d in range(1, tp):
        copy = remote(squares.at[t], squares.at[t], sq_send.at[d], sq_recv.at[d], tp_peer(d))
        copy.start()
        exchange.append(copy)
    l_mix.wait()
    scaled = (attended * mix_gain[...]).astype(BF16)
    l_wo.wait()
    branch[t] = mm(scaled, wo[...]).astype(BF16)
    for d in range(1, tp):
        copy = remote(branch.at[t], branch.at[t], br_send.at[d], br_recv.at[d], tp_peer(d))
        copy.start()
        exchange.append(copy)
    sent += exchange

    l_ffn.wait()
    l_experts.wait()
    l_weights.wait()
    l_wk.wait()
    l_wv.wait()
    new_keys[...] = mm(normed_in, wk[...]).astype(BF16)
    new_values[...] = mm(normed_in, wv[...]).astype(BF16)

    for copy in exchange:
        copy.wait_recv()
    head_total = squares[0][:, 0:1]
    summed = branch[0].astype(F32)
    for j in range(1, tp):
        head_total = head_total + squares[j][:, 0:1]
        summed = summed + branch[j].astype(F32)
    middle = whole + summed * lax.rsqrt(head_total / (tp * span) + eps)
    mid[...] = middle
    normed_mid = (
        middle * lax.rsqrt(jnp.mean(middle * middle, axis=1, keepdims=True) + eps) * ffn_gain[...]
    ).astype(BF16)
    tokens[0] = normed_mid

    direct = []
    for c in range(1, chips):
        copy = remote(
            tokens.at[0], tokens.at[2 * c], tok_send.at[c], tok_recv.at[c],
            {"ep": 2 * lax.rem(z + c, chips) + core},
        )
        copy.start()
        direct.append(copy)
    other = {"ep": 2 * z + 1 - core}
    forward = []
    for c in range(chips):
        copy = remote(tokens.at[2 * c], tokens.at[2 * c + 1], fwd_send.at[c], fwd_recv.at[c], other)
        if c:
            direct[c - 1].wait_recv()
        copy.start()
        forward.append(copy)
    sent += direct + forward
    l_gate.wait()
    l_up.wait()
    l_down.wait()
    for copy in forward:
        copy.wait_recv()
    inputs = jnp.concatenate([tokens[i].astype(F32) for i in range(ep)], axis=0).astype(BF16)
    gate = jnp.minimum(mm(inputs, gate_w[...]), limit)
    upper = jnp.clip(mm(inputs, up_w[...]), -limit, limit)
    active = ((upper + 1.0) * gate * jax.nn.sigmoid(alpha * gate)).astype(BF16)

    reduce = {}
    pair = 2 * seqs

    def send_piece(c, d):
        part = pl.ds(c * pair, pair)
        copy = remote(
            pieces.at[d, part], arrived.at[d, part], down_send.at[c, d], down_recv.at[c, d], tp_peer(d)
        )
        copy.start()
        reduce[c, d] = copy

    order = sorted(range(chips), key=lambda c: -min(c, chips - c))
    for d in list(range(1, tp)) + [0]:
        to = lax.rem(t + d, tp)
        columns = pl.ds(pl.multiple_of(to * shard, shard), shard)
        pieces[d] = mm(active, down_w[:, columns]).astype(BF16)
        if d:
            send_piece(order[0], d)
    for c in order[1:]:
        for d in range(1, tp):
            send_piece(c, d)
    weights = route_weights[...]
    share = weights / jnp.sum(weights, axis=0, keepdims=True)
    named = route_experts[...]
    diagonal = lax.broadcasted_iota(jnp.int32, (seqs, seqs), 0) == lax.broadcasted_iota(
        jnp.int32, (seqs, seqs), 1
    )
    factors = []
    for i in range(ep):
        expert = 2 * lax.rem(z + i // 2, chips) + (core if i % 2 == 0 else 1 - core)
        line = jnp.sum(jnp.where(named == expert, share, 0.0), axis=0, keepdims=True)
        factors.append(jnp.sum(jnp.where(diagonal, line, 0.0), axis=1, keepdims=True))
    returns = {}
    for c in order:
        part = pl.ds(c * pair, pair)
        result = pieces[0, part].astype(F32)
        for d in range(1, tp):
            reduce[c, d].wait_recv()
            result = result + arrived[d, part].astype(F32)
        for o in range(1, -1, -1):
            i = 2 * c + o
            block_rows = result[o * seqs:(o + 1) * seqs].astype(BF16)
            if i:
                outs[i] = block_rows
                home = 2 * lax.rem(z + chips - c, chips) + (core if o == 0 else 1 - core)
                copy = remote(outs.at[i], back.at[i], ret_send.at[i], ret_recv.at[i], {"ep": home})
                copy.start()
                returns[i] = copy
            else:
                back[0] = block_rows
    sent += list(reduce.values()) + list(returns.values())
    mixture = factors[0] * back[0].astype(F32)
    for c in order:
        for o in range(1, -1, -1):
            i = 2 * c + o
            if i:
                returns[i].wait_recv()
                mixture = mixture + factors[i] * back[i].astype(F32)
    own = mid[:, pl.ds(pl.multiple_of(t * shard, shard), shard)]
    mixed[...] = (own + mixture).astype(BF16)
    for copy in sent:
        copy.wait_send()


def hand_out(a, b, c, mixed, new_keys, new_values, sem):
    copies = [
        pltpu.make_async_copy(src, dst, sem.at[i])
        for i, (src, dst) in enumerate(((a, mixed), (b, new_keys), (c, new_values)))
    ]
    for copy in copies:
        copy.start()
    for copy in copies:
        copy.wait()


def body(
    tp, ep,
    resid, attn_gain, w_query, w_key, w_value, key_cache, value_cache, key_bias, lengths,
    mix_gain, w_out, ffn_gain, route_experts, route_weights, w_gate, w_up, w_down,
):
    seqs, heads, width, cache = key_cache.shape
    shard = resid.shape[1]
    model = tp * shard
    span = heads * width
    hidden = w_gate.shape[2]
    top = route_experts.shape[1]
    vmem = pl.BlockSpec(memory_space=pltpu.VMEM)
    hbm = pl.BlockSpec(memory_space=pl.ANY)
    dma = pltpu.SemaphoreType.DMA
    shapes = ((seqs, shard), (seqs, span), (seqs, span))
    held = pl.pallas_call(
        functools.partial(layer, tp, ep, heads, width),
        out_shape=tuple(pltpu.VMEM(shape, BF16) for shape in shapes),
        in_specs=[hbm] * 17,
        out_specs=(vmem, vmem, vmem),
        scratch_shapes=[
            pltpu.VMEM((seqs, shard), BF16),
            pltpu.VMEM((1, model), F32),
            pltpu.SMEM((seqs,), jnp.int32),
            pltpu.VMEM((1, span), F32),
            pltpu.VMEM((1, model), F32),
            pltpu.VMEM((top, seqs), jnp.int32),
            pltpu.VMEM((top, seqs), F32),
            pltpu.VMEM((model, span), BF16),
            pltpu.VMEM((seqs * span, cache), BF16),
            pltpu.VMEM((seqs, heads, cache), F32),
            pltpu.VMEM((seqs * span, cache), BF16),
            pltpu.VMEM((span, model), BF16),
            pltpu.VMEM((model, hidden), BF16),
            pltpu.VMEM((model, hidden), BF16),
            pltpu.VMEM((model, span), BF16),
            pltpu.VMEM((model, span), BF16),
            pltpu.VMEM((hidden, model), BF16),
            pltpu.VMEM((tp, seqs, shard), BF16),
            pltpu.VMEM((seqs * heads, cache), F32),
            pltpu.VMEM((tp, seqs, model), BF16),
            pltpu.VMEM((tp, seqs, 128), F32),
            pltpu.VMEM((seqs, model), F32),
            pltpu.VMEM((ep, seqs, model), BF16),
            pltpu.VMEM((tp, ep * seqs, shard), BF16),
            pltpu.VMEM((tp, ep * seqs, shard), BF16),
            pltpu.VMEM((ep, seqs, shard), BF16),
            pltpu.VMEM((ep, seqs, shard), BF16),
            dma((17,)),
            dma((tp,)), dma((tp,)), dma((tp,)), dma((tp,)), dma((tp,)), dma((tp,)),
            dma((ep,)), dma((ep,)), dma((ep,)), dma((ep,)),
            dma((ep // 2, tp)), dma((ep // 2, tp)), dma((ep,)), dma((ep,)),
        ],
        compiler_params=pltpu.CompilerParams(
            collective_id=0, has_side_effects=True, vmem_limit_bytes=60 * 1024 * 1024
        ),
    )(
        resid, attn_gain.reshape(1, -1), lengths, mix_gain.reshape(1, -1), ffn_gain.reshape(1, -1),
        route_experts.T, route_weights.T,
        w_query, key_cache.reshape(seqs * span, cache), key_bias, value_cache.reshape(seqs * span, cache),
        w_out, w_gate, w_up, w_key, w_value, w_down,
    )
    return pl.pallas_call(
        hand_out,
        out_shape=tuple(jax.ShapeDtypeStruct(shape, BF16) for shape in shapes),
        in_specs=[vmem] * 3,
        out_specs=(hbm,) * 3,
        scratch_shapes=[dma((3,))],
    )(*[pltpu.with_memory_space_constraint(x, pltpu.VMEM) for x in held])


def solution(mesh):
    placed = (
        P("ep", "tp"),
        P(),
        P(None, "tp"),
        P(None, "tp"),
        P(None, "tp"),
        P("ep", "tp", None, None),
        P("ep", "tp", None, None),
        P("ep", "tp", None),
        P("ep"),
        P("tp"),
        P("tp", None),
        P(),
        P("ep", None),
        P("ep", None),
        P("ep", None, "tp"),
        P("ep", None, "tp"),
        P("ep", "tp", None),
    )
    return jax.shard_map(
        functools.partial(body, mesh.shape["tp"], mesh.shape["ep"]),
        mesh=mesh,
        in_specs=placed,
        out_specs=(P("ep", "tp"), P("ep", "tp"), P("ep", "tp")),
        check_vma=False,
    )
```

profile of v0, /device:TPU:0, one launch (start us, length us, event | category | flops | bytes accessed | tf_op | source)
XLA Modules:
  0.0 33.4 jit_solution(1037619236527691104)
XLA Ops:
  0.6 32.2 %shard_map.184 = (bf16[8,512]{1,0:T(8,128)(2,1)S(1)}, bf16[8,256]{1,0:T(8,128)(2,1)S(1)}, bf16[8,256]{1,0:T(8,128)(2,1)S(1)}) custom-call(bf16[8,512]{1,0:T(8,128)(2,1)} %h_resid.1, f32[1,2048]{1,0:T(1,128)} %bitcast.9, s32[8]{0:T(128)} %h_lengths.1, f32[1,256]{1,0:T(1,128)} %bitcast.13, f32[1,2048]{1,0:T(1,128)} %bitcast.10, s32[4,8]{1,0:T(4,128)} %bitcast.11, ...), custom_call_target="tpu_custom_call" | custom-call | tf_op jit(solution)/shard_map/pallas_call | solution.py:309
  32.8 0.6 %shard_map.185 = (bf16[8,512]{1,0:T(8,128)(2,1)}, bf16[8,256]{1,0:T(8,128)(2,1)}, bf16[8,256]{1,0:T(8,128)(2,1)}) custom-call(bf16[8,512]{1,0:T(8,128)(2,1)S(1)} %get-tuple-element.6.a, bf16[8,256]{1,0:T(8,128)(2,1)S(1)} %get-tuple-element.7.b, bf16[8,256]{1,0:T(8,128)(2,1)S(1)} %get-tuple-element.8.c), custom_call_target="tpu_custom_call" | custom-call | tf_op jit(solution)/shard_map/pallas_call | solution.py:356
where the time goes:
time: 33.6 us; the launch traced here: 33.4 us
  Pallas kernels  32.8 us (98%)
  between operations  0.65 us (2%)
    pallas_call x1, Pallas kernels, body(): pl.pallas_call(functools.partial(layer, tp, ep, heads, width), out_shape=...  32.2 us

commit v1 on v0

v1 whole, which is shorter than its diff:
```python
import functools

import jax
import jax.numpy as jnp
from jax import lax
from jax.experimental import pallas as pl
from jax.experimental.pallas import tpu as pltpu
from jax.sharding import PartitionSpec as P

eps = 1e-06
limit = 7.0
alpha = 1.702
LIMIT_A = 48
LIMIT_B = 48
MESH = pl.DeviceIdType.MESH
F32 = jnp.float32
BF16 = jnp.bfloat16


def mm(a, b):
    return jnp.dot(a, b, preferred_element_type=F32)


def mm_nt(a, b):
    return lax.dot_general(a, b, (((1,), (1,)), ((), ())), preferred_element_type=F32)


def mm(a, b):
    return jnp.dot(a, b, preferred_element_type=F32)


def mm_nt(a, b):
    return lax.dot_general(a, b, (((1,), (1,)), ((), ())), preferred_element_type=F32)


_cur=[None]
def mark(name):
    if _cur[0] is not None:
        _cur[0].__exit__(None,None,None)
        _cur[0]=None
    if name:
        _cur[0]=jax.named_scope(name); _cur[0].__enter__()


def near_first(z, chips, k):
    if k == 0:
        return z
    room = jnp.minimum(z, chips - 1 - z)
    step = (k + 1) // 2
    both = z + step if k % 2 else z - step
    single = jnp.where(z < chips - 1 - z, z + (k - room), z - (k - room))
    return jnp.where(k <= 2 * room, both, single)


def peer_of(t, d, tp):
    if tp & (tp - 1):
        return lax.rem(t + d, tp)
    out = t
    bit = 1
    while bit < tp:
        if d & bit:
            out = out + bit - 2 * bit * lax.rem(out // bit, 2)
        bit *= 2
    return out


def start_loads(sem, groups):
    loads = []
    for i, group in enumerate(groups):
        copies = [pltpu.make_async_copy(src, dst, sem.at[i]) for src, dst in group]
        for copy in copies:
            copy.start()
        loads.append(copies)

    def loaded(i):
        for copy in loads[i]:
            copy.wait()

    return loaded


def gather(
    tp,
    h_resid, h_lengths, h_attn_gain, h_wq, h_key, h_value, h_bias,
    gathered, attn_gain, wq, key, value, bias_rows, limits,
    resid, lengths, bias, load_sem, send_sem, recv_sem,
):
    t = lax.axis_index("tp")
    seqs, heads, _ = bias.shape
    barrier = pltpu.get_barrier_semaphore()
    for d in range(1, tp):
        pl.semaphore_signal(barrier, inc=1, device_id={"tp": peer_of(t, d, tp)}, device_id_type=MESH)
    loaded = start_loads(load_sem, (
        ((h_resid, resid),),
        ((h_bias, bias), (h_lengths, lengths)),
        ((h_attn_gain, attn_gain), (h_wq, wq), (h_key, key), (h_value, value)),
    ))
    loaded(0)
    pl.semaphore_wait(barrier, tp - 1)

    def copy_to(d):
        return pltpu.make_async_remote_copy(
            src_ref=resid, dst_ref=gathered.at[t], send_sem=send_sem, recv_sem=recv_sem.at[d],
            device_id={"tp": peer_of(t, d, tp)}, device_id_type=MESH,
        )

    copies = [copy_to(d) for d in reversed(range(1, tp))]
    for copy in copies:
        copy.start()
    gathered[t] = resid[...]
    loaded(1)
    for n in range(seqs):
        bias_rows[pl.ds(n * heads, heads), :] = bias[n]
    row = lax.broadcasted_iota(jnp.int32, limits.shape, 0)
    limit_rows = jnp.zeros(limits.shape, jnp.int32)
    for n in range(seqs):
        limit_rows = jnp.where(row // heads == n, lengths[n], limit_rows)
    limits[...] = limit_rows
    loaded(2)
    for copy in copies:
        copy.wait_recv()
    for copy in copies:
        copy.wait_send()


def layer(
    tp, ep, heads, width,
    gathered, attn_gain, wq, key, value, bias_rows, limits,
    h_mix_gain, h_ffn_gain, h_experts, h_weights, h_wo, h_gate, h_up, h_wk, h_wv, h_down,
    mixed, new_keys, new_values,
    mix_gain, ffn_gain, route_experts, route_weights, wo, gate_w, up_w, wk, wv, down_w,
    branch, mid, tokens, pieces, arrived, outs, back,
    load_sem, send_sem, br_recv, tok_recv, fwd_recv, down_recv, ret_recv,
):
    t = lax.axis_index("tp")
    e = lax.axis_index("ep")
    chips = ep // 2
    z, core = e // 2, lax.rem(e, 2)
    _, seqs, shard = gathered.shape
    model = tp * shard
    span = heads * width
    rows = seqs * heads
    cache = key.shape[1]

    def tp_peer(d):
        return {"tp": peer_of(t, d, tp)}

    def ep_peer(d):
        return {"ep": lax.rem(e + d, ep)}

    sent = []

    def remote(src, dst, recv, device):
        return pltpu.make_async_remote_copy(
            src_ref=src, dst_ref=dst, send_sem=send_sem, recv_sem=recv, device_id=device, device_id_type=MESH
        )

    def send(src, dst, recv, device):
        copy = remote(src, dst, recv, device)
        copy.start()
        sent.append(copy)
        return copy

    barrier = pltpu.get_barrier_semaphore()
    for d in range(1, ep):
        pl.semaphore_signal(barrier, inc=1, device_id=ep_peer(d), device_id_type=MESH)
    for d in range(1, tp):
        pl.semaphore_signal(barrier, inc=1, device_id=tp_peer(d), device_id_type=MESH)
    loaded = start_loads(load_sem, (
        ((h_mix_gain, mix_gain), (h_wo, wo)),
        ((h_ffn_gain, ffn_gain), (h_experts, route_experts), (h_weights, route_weights), (h_wk, wk), (h_wv, wv)),
        ((h_gate.at[0], gate_w), (h_up.at[0], up_w), (h_down.at[0], down_w)),
    ))

    live = lax.broadcasted_iota(jnp.int32, (rows, cache), 1) < limits[:, 0:1]
    own_row = lax.broadcasted_iota(jnp.int32, (rows, span), 0)
    own_head = lax.broadcasted_iota(jnp.int32, (rows, span), 1) // width
    repeat = (
        lax.broadcasted_iota(jnp.int32, (rows, seqs), 0) // heads
        == lax.broadcasted_iota(jnp.int32, (rows, seqs), 1)
    ).astype(F32).astype(BF16)
    block = min(256, cache)
    blocks = cache // block
    lower = (
        lax.broadcasted_iota(jnp.int32, (block, block), 0)
        >= lax.broadcasted_iota(jnp.int32, (block, block), 1)
    ).astype(F32).astype(BF16)

    whole = jnp.concatenate([gathered[j].astype(F32) for j in range(tp)], axis=1)
    normed_in = (
        whole * lax.rsqrt(jnp.mean(whole * whole, axis=1, keepdims=True) + eps) * attn_gain[...]
    ).astype(BF16)
    query = mm(normed_in, wq[...]).astype(BF16)

    spread = mm(repeat, query)
    masked = jnp.concatenate(
        [jnp.where(own_row == n * heads + own_head, spread, 0.0).astype(BF16) for n in range(seqs)], axis=1
    )
    scores = mm(masked, key[...]) * width ** (-0.5) + bias_rows[...]
    soft = jnp.maximum(scores, 0.0) + jnp.log1p(jnp.exp(-jnp.abs(scores)))
    soft = jnp.where(live, soft, 0.0)
    stacked = jnp.concatenate([soft[:, b * block:(b + 1) * block] for b in range(blocks)], axis=0)
    high = stacked.astype(BF16)
    rest = stacked - high.astype(F32)
    middle_part = rest.astype(BF16)
    low = (rest - middle_part.astype(F32)).astype(BF16)
    within = mm(high, lower) + mm(middle_part, lower) + mm(low, lower)
    later = jnp.zeros((rows, 1), F32)
    suffix = [None] * blocks
    for b in reversed(range(blocks)):
        part = within[b * rows:(b + 1) * rows]
        suffix[b] = part + later
        later = later + part[:, 0:1]
    suffix = jnp.concatenate(suffix, axis=1)
    stick = jnp.where(live, jnp.exp(scores - suffix), 0.0).astype(BF16)

    seq_row = lax.broadcasted_iota(jnp.int32, (seqs, span), 0)
    attended = jnp.zeros((seqs, span), F32)
    whole_product = mm_nt(stick, value[...])
    for n in range(seqs):
        product = whole_product[:, n * span:(n + 1) * span]
        product = jnp.where(own_row == n * heads + own_head, product, 0.0)
        attended = jnp.where(seq_row == n, jnp.sum(product, axis=0, keepdims=True), attended)

    square = jnp.sum(attended * attended, axis=1, keepdims=True)
    lane = lax.broadcasted_iota(jnp.int32, (seqs, 128), 1)
    tail = jnp.zeros((seqs, 128), F32)
    for i in range(3):
        digit = square.astype(BF16).astype(F32)
        tail = jnp.where(lane == i, digit, tail)
        square = square - digit
    loaded(0)
    scaled = (attended * mix_gain[...]).astype(BF16)
    branch[t, :, pl.ds(model, 128)] = tail.astype(BF16)
    branch[t, :, pl.ds(0, model)] = mm(scaled, wo[...]).astype(BF16)
    pl.semaphore_wait(barrier, tp + ep - 2)
    exchange = [send(branch.at[t], branch.at[t], br_recv.at[d], tp_peer(d)) for d in reversed(range(1, tp))]

    loaded(1)
    new_keys[...] = mm(normed_in, wk[...]).astype(BF16)
    new_values[...] = mm(normed_in, wv[...]).astype(BF16)
    weights = route_weights[...]
    share = weights / jnp.sum(weights, axis=0, keepdims=True)
    named = route_experts[...]
    diagonal = lax.broadcasted_iota(jnp.int32, (seqs, seqs), 0) == lax.broadcasted_iota(
        jnp.int32, (seqs, seqs), 1
    )
    factors = []
    for x in range(ep):
        line = jnp.sum(jnp.where(named == x, share, 0.0), axis=0, keepdims=True)
        factors.append(jnp.sum(jnp.where(diagonal, line, 0.0), axis=1, keepdims=True))

    for copy in exchange:
        copy.wait_recv()
    head_total = jnp.zeros((seqs, 1), F32)
    summed = jnp.zeros((seqs, model), F32)
    for j in range(tp):
        head_total = head_total + jnp.sum(branch[j, :, pl.ds(model, 128)].astype(F32), axis=1, keepdims=True)
        summed = summed + branch[j, :, pl.ds(0, model)].astype(F32)
    middle = whole + summed * lax.rsqrt(head_total / (tp * span) + eps)
    mid[...] = middle
    normed_mid = (
        middle * lax.rsqrt(jnp.mean(middle * middle, axis=1, keepdims=True) + eps) * ffn_gain[...]
    ).astype(BF16)
    tokens[z, core] = normed_mid

    nearest = [near_first(z, chips, k) for k in range(chips)]
    other = {"ep": 2 * z + 1 - core}
    for k in reversed(range(1, chips)):
        send(tokens.at[z, core], tokens.at[z, core], tok_recv.at[z], {"ep": 2 * nearest[k] + core})
    send(tokens.at[z, core], tokens.at[z, core], fwd_recv.at[z], other)

    for k in range(1, chips):
        s = nearest[k]
        remote(tokens.at[s, core], tokens.at[s, core], tok_recv.at[s], other).wait_recv()
        send(tokens.at[s, core], tokens.at[s, core], fwd_recv.at[s], other)
    loaded(2)
    for k in range(chips):
        s = nearest[k]
        remote(tokens.at[s, 1 - core], tokens.at[s, 1 - core], fwd_recv.at[s], other).wait_recv()
    far = list(reversed(range(chips)))
    inputs = jnp.concatenate([tokens[nearest[k], o].astype(F32) for k in far for o in range(2)], axis=0).astype(BF16)
    gate = jnp.minimum(mm(inputs, gate_w[...]), limit)
    upper = jnp.clip(mm(inputs, up_w[...]), -limit, limit)
    active = ((upper + 1.0) * gate * jax.nn.sigmoid(alpha * gate)).astype(BF16)
    pair = 2 * seqs
    reduce = {}

    def send_piece(i, d):
        part = pl.ds(i * pair, pair)
        reduce[i, d] = send(pieces.at[d, part], arrived.at[d, part], down_recv.at[i, d], tp_peer(d))

    for d in list(reversed(range(1, tp))) + [0]:
        to = peer_of(t, d, tp)
        columns = pl.ds(pl.multiple_of(to * shard, shard), shard)
        pieces[d] = mm(active, down_w[:, columns]).astype(BF16)
        if d:
            send_piece(0, d)
    for i in range(1, chips):
        for d in reversed(range(1, tp)):
            send_piece(i, d)
    for i, k in enumerate(far):
        part = pl.ds(i * pair, pair)
        result = pieces[0, part].astype(F32)
        for d in range(1, tp):
            reduce[i, d].wait_recv()
        for d in range(1, tp):
            result = result + arrived[d, part].astype(F32)
        for o in range(2):
            outs[k, o] = result[o * seqs:(o + 1) * seqs].astype(BF16)
        if k:
            for o in range(2):
                send(outs.at[k, o], back.at[e], ret_recv.at[e], {"ep": 2 * nearest[k] + o})
        else:
            send(outs.at[0, 1 - core], back.at[e], ret_recv.at[e], other)
            back[e] = outs[0, core]

    for i in range(1, ep):
        x = lax.rem(e + i, ep)
        remote(outs.at[0, 0], back.at[x], ret_recv.at[x], other).wait_recv()
    mixture = mid[:, pl.ds(pl.multiple_of(t * shard, shard), shard)]
    for x in range(ep):
        mixture = mixture + factors[x] * back[x].astype(F32)
    mixed[...] = mixture.astype(BF16)
    for copy in sent:
        copy.wait_send()


def hand_out(a, b, c, mixed, new_keys, new_values, sem):
    copies = [
        pltpu.make_async_copy(src, dst, sem.at[i])
        for i, (src, dst) in enumerate(((a, mixed), (b, new_keys), (c, new_values)))
    ]
    for copy in copies:
        copy.start()
    for copy in copies:
        copy.wait()


def body(
    tp, ep,
    resid, attn_gain, w_query, w_key, w_value, key_cache, value_cache, key_bias, lengths,
    mix_gain, w_out, ffn_gain, route_experts, route_weights, w_gate, w_up, w_down,
):
    seqs, heads, width, cache = key_cache.shape
    shard = resid.shape[1]
    model = tp * shard
    span = heads * width
    hidden = w_gate.shape[2]
    top = route_experts.shape[1]
    chips = ep // 2
    vmem = pl.BlockSpec(memory_space=pltpu.VMEM)
    hbm = pl.BlockSpec(memory_space=pl.ANY)
    dma = pltpu.SemaphoreType.DMA
    shapes = ((seqs, shard), (seqs, span), (seqs, span))
    keep = (
        ((tp, seqs, shard), BF16),
        ((1, model), F32),
        ((model, span), BF16),
        ((seqs * span, cache), BF16),
        ((seqs * span, cache), BF16),
        ((seqs * heads, cache), F32),
        ((seqs * heads, 128), jnp.int32),
    )
    first = pl.pallas_call(
        functools.partial(gather, tp),
        out_shape=tuple(pltpu.VMEM(*x) for x in keep),
        in_specs=[hbm] * 7,
        out_specs=(vmem,) * 7,
        scratch_shapes=[
            pltpu.VMEM((seqs, shard), BF16),
            pltpu.SMEM((seqs,), jnp.int32),
            pltpu.VMEM((seqs, heads, cache), F32),
            dma((3,)), dma, dma((tp,)),
        ],
        compiler_params=pltpu.CompilerParams(
            collective_id=0, has_side_effects=True, vmem_limit_bytes=LIMIT_A * 1024 * 1024
        ),
    )(
        resid, lengths, attn_gain.reshape(1, -1), w_query, key_cache.reshape(seqs * span, cache),
        value_cache.reshape(seqs * span, cache), key_bias,
    )
    held = pl.pallas_call(
        functools.partial(layer, tp, ep, heads, width),
        out_shape=tuple(pltpu.VMEM(shape, BF16) for shape in shapes),
        in_specs=[vmem] * 7 + [hbm] * 10,
        out_specs=(vmem, vmem, vmem),
        scratch_shapes=[
            pltpu.VMEM((1, span), F32),
            pltpu.VMEM((1, model), F32),
            pltpu.VMEM((top, seqs), jnp.int32),
            pltpu.VMEM((top, seqs), F32),
            pltpu.VMEM((span, model), BF16),
            pltpu.VMEM((model, hidden), BF16),
            pltpu.VMEM((model, hidden), BF16),
            pltpu.VMEM((model, span), BF16),
            pltpu.VMEM((model, span), BF16),
            pltpu.VMEM((hidden, model), BF16),
            pltpu.VMEM((tp, seqs, model + 128), BF16),
            pltpu.VMEM((seqs, model), F32),
            pltpu.VMEM((chips, 2, seqs, model), BF16),
            pltpu.VMEM((tp, ep * seqs, shard), BF16),
            pltpu.VMEM((tp, ep * seqs, shard), BF16),
            pltpu.VMEM((chips, 2, seqs, shard), BF16),
            pltpu.VMEM((ep, seqs, shard), BF16),
            dma((3,)), dma, dma((tp,)), dma((chips,)), dma((chips,)), dma((chips, tp)), dma((ep,)),
        ],
        compiler_params=pltpu.CompilerParams(
            collective_id=1, has_side_effects=True, vmem_limit_bytes=LIMIT_B * 1024 * 1024
        ),
    )(
        *[pltpu.with_memory_space_constraint(x, pltpu.VMEM) for x in first],
        mix_gain.reshape(1, -1), ffn_gain.reshape(1, -1), route_experts.T, route_weights.T,
        w_out, w_gate, w_up, w_key, w_value, w_down,
    )
    return pl.pallas_call(
        hand_out,
        out_shape=tuple(jax.ShapeDtypeStruct(shape, BF16) for shape in shapes),
        in_specs=[vmem] * 3,
        out_specs=(hbm,) * 3,
        scratch_shapes=[dma((3,))],
    )(*[pltpu.with_memory_space_constraint(x, pltpu.VMEM) for x in held])


def solution(mesh):
    placed = (
        P("ep", "tp"),
        P(),
        P(None, "tp"),
        P(None, "tp"),
        P(None, "tp"),
        P("ep", "tp", None, None),
        P("ep", "tp", None, None),
        P("ep", "tp", None),
        P("ep"),
        P("tp"),
        P("tp", None),
        P(),
        P("ep", None),
        P("ep", None),
        P("ep", None, "tp"),
        P("ep", None, "tp"),
        P("ep", "tp", None),
    )
    return jax.shard_map(
        functools.partial(body, mesh.shape["tp"], mesh.shape["ep"]),
        mesh=mesh,
        in_specs=placed,
        out_specs=(P("ep", "tp"), P("ep", "tp"), P("ep", "tp")),
        check_vma=False,
    )
```

time: 33.6 us -> 30.2 us (0.90)
  Pallas kernels: 32.8 us -> 29.3 us
    pallas_call x1, Pallas kernels: 32.2 us -> 22.3 us  [body(): pl.pallas_call(functools.partial(layer, tp, ep, heads, width), out_shape=...]
    pallas_call x0 -> x1, Pallas kernels: none -> 6.39 us  [body(): pl.pallas_call(functools.partial(gather, tp), out_shape=tuple((pltpu.VMEM...]
where the time goes in v1:
time: 30.2 us; the launch traced here: 30 us
  Pallas kernels  29.3 us (97%)
  between operations  0.65 us (2%)
    pallas_call x1, Pallas kernels, body(): pl.pallas_call(functools.partial(layer, tp, ep, heads, width), out_shape=...  22.3 us
    pallas_call x1, Pallas kernels, body(): pl.pallas_call(functools.partial(gather, tp), out_shape=tuple((pltpu.VMEM...  6.39 us
    pallas_call x1, Pallas kernels, body(): pl.pallas_call(hand_out, out_shape=tuple((jax.ShapeDtypeStruct(shape, BF1...  0.63 us

profile of v1, /device:TPU:0, one launch (start us, length us, event | category | flops | bytes accessed | tf_op | source)
XLA Modules:
  0.0 30.0 jit_solution(13336826851316205204)
XLA Ops:
  0.6 6.4 %shard_map.184 = (bf16[4,8,512]{2,1,0:T(8,128)(2,1)S(1)}, f32[1,2048]{1,0:T(1,128)S(1)}, bf16[2048,256]{1,0:T(8,128)(2,1)S(1)}, bf16[2048,1024]{1,0:T(8,128)(2,1...) custom-call(bf16[8,512]{1,0:T(8,128)(2,1)} %h_resid.1, s32[8]{0:T(128)} %h_lengths.1, ...), custom_call_target="tpu_custom_call" | custom-call | tf_op jit(solution)/shard_map/pallas_call | solution.py:365
  7.0 22.3 %shard_map.185 = (bf16[8,512]{1,0:T(8,128)(2,1)S(1)}, bf16[8,256]{1,0:T(8,128)(2,1)S(1)}, bf16[8,256]{1,0:T(8,128)(2,1)S(1)}) custom-call(bf16[4,8,512]{2,1,0:T(8,128)(2,1)S(1)} %get-tuple-element.13.gathered, f32[1,2048]{1,0:T(1,128)S(1)} %get-tuple-element.14.attn_gain, bf16[2048,256]{1,0:T(8,128)(2,1)S(1)} %get-tuple-element.15.wq, ...), custom_call_target="tpu_custom_call" | custom-call | tf_op jit(solution)/shard_map/pallas_call | solution.py:383
  29.4 0.6 %shard_map.186 = (bf16[8,512]{1,0:T(8,128)(2,1)}, bf16[8,256]{1,0:T(8,128)(2,1)}, bf16[8,256]{1,0:T(8,128)(2,1)}) custom-call(bf16[8,512]{1,0:T(8,128)(2,1)S(1)} %get-tuple-element.20.a, bf16[8,256]{1,0:T(8,128)(2,1)S(1)} %get-tuple-element.21.b, bf16[8,256]{1,0:T(8,128)(2,1)S(1)} %get-tuple-element.22.c), custom_call_target="tpu_custom_call" | custom-call | tf_op jit(solution)/shard_map/pallas_call | solution.py:416
